TPU v7x, 32 devices: a whole 2x2x4 slice. The times are simulated.
32 devices in a mesh: grp: 2 (over y), kv: 4 (over z), tp: 4 (over x, core).
Axes of the slice: x: 2, y: 2, z: 4, core: 2. Of those that a mesh axis runs over, the one named last changes fastest.
Arguments:
- tokens: bfloat16 [64, 4096], P('grp', ('kv', 'tp')), parts along dimension 0, may hold values from -12 to 12
- gain_in: float32 [4096], P('kv'), may hold values from 0.1 to 1.9
- w_query: bfloat16 [4096, 1024], P('kv', 'tp'), may hold values from -0.09375 to 0.09375
- w_key: bfloat16 [4096, 1024], P('kv', 'tp'), may hold values from -0.09375 to 0.09375
- w_value: bfloat16 [4096, 2048], P('kv', 'tp'), may hold values from -0.09375 to 0.09375
- w_outgate: bfloat16 [4096, 2048], P('kv', 'tp'), may hold values from -0.09375 to 0.09375
- w_input_gate: bfloat16 [4096, 16], P('kv'), may hold values from -0.09375 to 0.09375
- w_forget_gate: bfloat16 [4096, 16], P('kv'), may hold values from -0.09375 to 0.09375
- bias_input: float32 [16], replicated, may hold values from -1 to 1
- bias_forget: float32 [16], replicated, may hold values from -1 to 4
- cell_state: float32 [64, 16, 64, 128], P(('grp', 'kv'), 'tp'), parts along dimension 0, may hold values from -6 to 6
- norm_state: float32 [64, 16, 64], P(('grp', 'kv'), 'tp'), parts along dimension 0, may hold values from -18 to 18
- max_state: float32 [64, 16], P(('grp', 'kv'), 'tp'), parts along dimension 0, may hold values from -1 to 2
- w_proj: bfloat16 [2048, 4096], P('tp', 'kv'), may hold values from -0.125 to 0.125
- gain_mid: float32 [4096], P('kv'), may hold values from 0.1 to 1.9
- w_up: bfloat16 [4096, 16384], P('kv', 'tp'), may hold values from -0.09375 to 0.09375
- w_down: bfloat16 [16384, 4096], P('tp', 'kv'), may hold values from -0.046875 to 0.046875
Outputs:
- mixed: bfloat16 [64, 4096], P('grp', ('kv', 'tp')), parts along dimension 0
- cell_new: float32 [64, 16, 64, 128], P(('grp', 'kv'), 'tp'), parts along dimension 0
- norm_new: float32 [64, 16, 64], P(('grp', 'kv'), 'tp'), parts along dimension 0
- max_new: float32 [64, 16], P(('grp', 'kv'), 'tp'), parts along dimension 0
There are 2 independent parts, one for each index of `grp`. A program takes and returns all parts, laid end to end along the dimension named above; an argument that names none is the same for every part. Nothing has to cross between parts.
All inputs are finite; a program needn't handle non-finite values.
Results may differ from a plain program's by a relative error of at most 0.015.
Values may be sent and summed in bfloat16 or wider, within the bound.
A program may use at most 64 MiB of HBM per device.

v0:
```python
import jax
import jax.numpy as jnp
from jax import lax
from jax.sharding import PartitionSpec as P

D = 4096


EPSILON = 1e-06


def memory_step(
    query, keys, values, outgate, log_input, log_forget, cell_state, norm_state, max_state
):
    max_new = jnp.maximum(log_forget + max_state, log_input)
    keep = jnp.exp(log_forget + max_state - max_new)
    write = jnp.exp(log_input - max_new)
    cell_new = (
        keep[..., None, None] * cell_state
        + (write[..., None] * keys)[..., :, None] * values[..., None, :]
    )
    norm_new = keep[..., None] * norm_state + write[..., None] * keys
    numer = jnp.einsum("shk,shkv->shv", query, cell_new, precision=lax.Precision.HIGHEST)
    denom = jnp.maximum(jnp.abs(jnp.sum(query * norm_new, axis=-1)), jnp.exp(-max_new))
    heads = (jax.nn.sigmoid(outgate) * numer / denom[..., None]).astype(jnp.bfloat16)
    return (heads, cell_new, norm_new, max_new)


def matmul(left, right):
    return jnp.dot(left, right, preferred_element_type=jnp.float32)


def on_device(
    tokens,
    gain_in,
    w_query,
    w_key,
    w_value,
    w_outgate,
    w_input_gate,
    w_forget_gate,
    bias_input,
    bias_forget,
    cell_state,
    norm_state,
    max_state,
    w_proj,
    gain_mid,
    w_up,
    w_down,
):
    seq_local, head_count = (cell_state.shape[0], cell_state.shape[1])
    key_dim, value_dim = (cell_state.shape[2], cell_state.shape[3])
    head_start = lax.axis_index("tp") * head_count
    column_width = tokens.shape[1]
    gathered = lax.all_gather(tokens, "tp", axis=1, tiled=True)
    widef = gathered.astype(jnp.float32)
    part_squares = jnp.sum(widef * widef, axis=1)
    normed = (widef * gain_in).astype(jnp.bfloat16)
    gate_input = lax.dynamic_slice_in_dim(w_input_gate, head_start, head_count, 1)
    gate_forget = lax.dynamic_slice_in_dim(w_forget_gate, head_start, head_count, 1)
    terms = jnp.concatenate(
        [
            matmul(normed, w_query),
            matmul(normed, w_key),
            matmul(normed, w_value),
            matmul(normed, w_outgate),
            matmul(normed, gate_input),
            matmul(normed, gate_forget),
        ],
        axis=1,
    )
    total_squares = lax.psum(part_squares, "kv")
    own_terms = lax.psum_scatter(terms, "kv", scatter_dimension=0, tiled=True)
    row_squares = lax.dynamic_slice_in_dim(
        total_squares, lax.axis_index("kv") * seq_local, seq_local, 0
    )
    own_terms = own_terms * lax.rsqrt(row_squares / D + EPSILON)[:, None]
    width_qk = head_count * key_dim
    width_v = head_count * value_dim
    query = own_terms[:, :width_qk].reshape(seq_local, head_count, key_dim) * key_dim ** (-0.5)
    keys = own_terms[:, width_qk : 2 * width_qk].reshape(seq_local, head_count, key_dim)
    offset = 2 * width_qk
    values = own_terms[:, offset : offset + width_v].reshape(seq_local, head_count, value_dim)
    offset = offset + width_v
    outgate = own_terms[:, offset : offset + width_v].reshape(seq_local, head_count, value_dim)
    offset = offset + width_v
    log_input = own_terms[:, offset : offset + head_count] + lax.dynamic_slice_in_dim(
        bias_input, head_start, head_count, 0
    )
    offset = offset + head_count
    log_forget = jax.nn.log_sigmoid(
        own_terms[:, offset : offset + head_count]
        + lax.dynamic_slice_in_dim(bias_forget, head_start, head_count, 0)
    )
    heads, cell_new, norm_new, max_new = memory_step(
        query, keys, values, outgate, log_input, log_forget, cell_state, norm_state, max_state
    )
    branch_part = matmul(
        lax.all_gather(heads.reshape(seq_local, width_v), "kv", axis=0, tiled=True), w_proj
    )
    branch = lax.psum(branch_part, "tp")
    middle = (widef + branch).astype(jnp.bfloat16)
    midf = middle.astype(jnp.float32)
    mid_squares = jnp.sum(midf * midf, axis=1)
    normed_mid = (midf * gain_mid).astype(jnp.bfloat16)
    up_part = matmul(normed_mid, w_up)
    up_rows, square_rows = (
        lax.psum_scatter(up_part, "kv", scatter_dimension=0, tiled=True),
        lax.psum_scatter(mid_squares, "kv", scatter_dimension=0, tiled=True),
    )
    upward = up_rows * lax.rsqrt(square_rows / D + EPSILON)[:, None]
    hidden = jnp.square(jax.nn.relu(upward)).astype(jnp.bfloat16)
    down_part = matmul(lax.all_gather(hidden, "kv", axis=0, tiled=True), w_down)
    own_down = lax.psum_scatter(
        down_part.astype(jnp.bfloat16), "tp", scatter_dimension=1, tiled=True
    ).astype(jnp.float32)
    residual = lax.dynamic_slice_in_dim(midf, lax.axis_index("tp") * column_width, column_width, 1)
    mixed = (residual + own_down).astype(jnp.bfloat16)
    return (mixed, cell_new, norm_new, max_new)


def solution(mesh):
    in_specs = (
        P("grp", ("kv", "tp")),
        P("kv"),
        P("kv", "tp"),
        P("kv", "tp"),
        P("kv", "tp"),
        P("kv", "tp"),
        P("kv", None),
        P("kv", None),
        P(),
        P(),
        P(("grp", "kv"), "tp", None, None),
        P(("grp", "kv"), "tp", None),
        P(("grp", "kv"), "tp"),
        P("tp", "kv"),
        P("kv"),
        P("kv", "tp"),
        P("tp", "kv"),
    )
    out_specs = (
        P("grp", ("kv", "tp")),
        P(("grp", "kv"), "tp", None, None),
        P(("grp", "kv"), "tp", None),
        P(("grp", "kv"), "tp"),
    )
    return jax.shard_map(
        on_device, mesh=mesh, in_specs=in_specs, out_specs=out_specs, check_vma=False
    )
```

profile of v0, /device:TPU:0, one launch (start us, length us, event | category | flops | bytes accessed | tf_op | source)
XLA Modules:
  0.0 185.4 jit_solution(15501665608441207515)
XLA Ops:
  7.2 0.0 all-reduce.7.cloned.1.call-start
  7.2 6.6 %all_gather.9 = bf16[32,1024]{1,0:T(8,128)(2,1)S(1)} all-gather(bf16[32,256]{1,0:T(8,128)(2,1)} %param.17), channel_id=1, replica_groups=mesh['grp'=2,'kv'=4,'tp'=4] {'tp'}, dimensions={1}, use_global_device_ids=true | all-gather | bytes 81920 | tf_op jit(solution)/shard_map/all_gather | solution.py:56
  13.8 0.9 fusion.8
  14.7 0.9 fusion.6
  15.6 1.3 fusion.14
  16.8 1.2 fusion.16
  18.1 1.5 fusion.12
  19.6 1.5 fusion.10
  21.1 0.8 concatenate.3
  21.9 0.0 all-reduce.7.cloned.1.call-update
  21.9 0.0 all-reduce.5.cloned.1.call-start
  22.0 0.7 dynamic_slice.22
  22.7 0.7 dynamic_slice.21
  23.5 0.8 copy.29
  24.2 1.2 dynamic-slice
  26.1 0.1 fusion.1
  26.2 12.5 %psum.14 = f32[32]{0:T(128)S(1)} all-reduce(f32[32]{0:T(128)S(1)} %fusion.1), channel_id=1, replica_groups=mesh['grp'=2,'kv'=4,'tp'=4] {'kv'}, use_global_device_ids=true, to_apply=%region_2.0 | all-reduce | flops 32 | bytes 256 | tf_op jit(solution)/shard_map/psum | solution.py:73
  38.7 0.1 add_rsqrt_fusion
  38.8 20.1 %all-reduce.7.cloned.1.call-done = f32[32,1544]{1,0:T(8,128)} async-done(((f32[32,1544]{1,0:T(8,128)}), f32[32,1544]{1,0:T(8,128)}) %all-reduce.7.cloned.1.call-update) | async-done | bytes 197648
  58.8 0.9 dynamic-slice_multiply_fusion
  59.7 0.1 reshape.42
  59.8 0.1 mul.118
  59.9 0.1 subtract_exponential_fusion.1
  60.0 0.1 reshape.40
  60.1 1.4 multiply_reduce_fusion.1
  61.5 0.1 copy.31
  61.6 1.6 multiply_add_fusion
  63.2 1.0 fusion.39
  64.2 0.1 fusion.27
  64.3 13.2 %all_gather.10 = bf16[32,512]{1,0:T(8,128)(2,1)S(1)} all-gather(bf16[8,512]{1,0:T(8,128)(2,1)S(1)} %fusion.27), channel_id=1, replica_groups=mesh['grp'=2,'kv'=4,'tp'=4] {'kv'}, dimensions={0}, use_global_device_ids=true | all-gather | bytes 40960 | tf_op jit(solution)/shard_map/all_gather | solution.py:100
  77.5 0.9 fusion.40
  78.4 0.0 all-reduce.5.cloned.1.call-update
  78.4 0.0 reduce-scatter.3.cloned.1.call-start
  78.5 31.8 %all-reduce.5.cloned.1.call-done = f32[32,1024]{1,0:T(8,128)} async-done(((f32[32,1024]{1,0:T(8,128)}), f32[32,1024]{1,0:T(8,128)}) %all-reduce.5.cloned.1.call-update) | async-done | bytes 131088 | tf_op jit(solution)/shard_map/psum | solution.py:102
  110.3 1.0 multiply_reduce_fusion
  111.4 5.7 %fusion.3 = f32[32,4096]{1,0:T(8,128)} fusion(bf16[1024,4096]{1,0:T(8,128)(2,1)} %param.32, f32[32,1024]{1,0:T(8,128)S(1)} %get-tuple-element.13, f32[1024]{0:T(1024)S(1)} %copy-done.2), kind=kOutput, calls=%fused_computation.11 | convolution fusion | flops 268500992 | bytes 9048064 | tf_op jit(solution)/shard_map/dot_general | solution.py:30
  117.1 0.0 reduce-scatter.3.cloned.1.call-update
  117.1 0.0 reduce-scatter.5.cloned.1.call-start
  117.2 11.9 %all-reduce.1 = f32[32]{0:T(128)S(1)} all-reduce(f32[32]{0:T(128)S(1)} %get-tuple-element.12), channel_id=4, replica_groups=mesh['grp'=2,'kv'=4,'tp'=4] {'kv'}, use_global_device_ids=true, to_apply=%region_7.8.clone | all-reduce | flops 32 | bytes 256
  129.0 0.1 fusion.35
  129.1 10.1 %reduce-scatter.3.cloned.1.call-done = f32[8,4096]{1,0:T(8,128)} async-done(((f32[32,4096]{1,0:T(8,128)}), f32[8,4096]{1,0:T(8,128)}) %reduce-scatter.3.cloned.1.call-update) | async-done | bytes 131088 | tf_op jit(solution)/shard_map/reduce_scatter | solution.py:109
  139.2 1.0 multiply_convert_fusion
  140.2 14.0 %all_gather.11 = bf16[32,4096]{1,0:T(8,128)(2,1)S(1)} all-gather(bf16[8,4096]{1,0:T(8,128)(2,1)S(1)} %multiply_convert_fusion), channel_id=1, replica_groups=mesh['grp'=2,'kv'=4,'tp'=4] {'kv'}, dimensions={0}, use_global_device_ids=true | all-gather | bytes 327680 | tf_op jit(solution)/shard_map/all_gather | solution.py:114
  154.2 5.6 %convolution_convert_fusion = bf16[32,1024]{1,0:T(8,128)(2,1)} fusion(bf16[32,4096]{1,0:T(8,128)(2,1)S(1)} %all_gather.11, bf16[4096,1024]{1,0:T(8,128)(2,1)} %param.33), kind=kOutput, calls=%fused_computation | convolution fusion | flops 268468224 | bytes 8716288 | tf_op jit(solution)/shard_map/dot_general | solution.py:30
  159.7 0.0 reduce-scatter.5.cloned.1.call-update
  159.8 0.7 copy.32
  160.4 17.1 %reduce-scatter.5.cloned.1.call-done = bf16[32,256]{1,0:T(8,128)(2,1)} async-done(((bf16[32,1024]{1,0:T(8,128)(2,1)}), bf16[32,256]{1,0:T(8,128)(2,1)}) %reduce-scatter.5.cloned.1.call-update) | async-done | bytes 16400 | tf_op jit(solution)/shard_map/reduce_scatter | solution.py:115
  177.5 1.3 add_convert_fusion
  (11 shorter events, 0.0 us)
Async XLA Ops:
  7.2 70.3 %copy-start = (bf16[512,1024]{1,0:T(8,128)(2,1)S(1)}, bf16[512,1024]{1,0:T(8,128)(2,1)}, u32[]{:S(2)}) copy-start(bf16[512,1024]{1,0:T(8,128)(2,1)} %param.30) | copy-start | bytes 3145732
  7.2 104.2 %copy-start.2 = (f32[1024]{0:T(1024)S(1)}, f32[1024]{0:T(1024)}, u32[]{:S(2)}) copy-start(f32[1024]{0:T(1024)} %param.31) | copy-start | bytes 12292
  7.2 51.6 %all-reduce.7.cloned.1.call-start = ((), (), s32[]{:S(2)}) async-start(), calls=%async_computation.5 | async-start | bytes 425984
  21.9 88.4 %all-reduce.5.cloned.1.call-start = ((), (), s32[]{:S(2)}) async-start(), calls=%async_computation.2 | async-start | bytes 262144 | tf_op jit(solution)/shard_map/psum | solution.py:102
  63.2 53.9 %copy-start.1 = (f32[8,4,64,128]{3,2,1,0:T(8,128)}, f32[8,4,64,128]{3,2,1,0:T(8,128)S(1)}, u32[]{:S(2)}) copy-start(f32[8,4,64,128]{3,2,1,0:T(8,128)S(1)} %multiply_add_fusion) | copy-start | bytes 3145732
  78.4 60.7 %reduce-scatter.3.cloned.1.call-start = ((), (), s32[]{:S(2)}) async-start(), calls=%async_computation.3 | async-start | bytes 655360 | tf_op jit(solution)/shard_map/reduce_scatter | solution.py:109
  117.1 60.4 %reduce-scatter.5.cloned.1.call-start = ((), (), s32[]{:S(2)}) async-start(), calls=%async_computation.4 | async-start | bytes 81920 | tf_op jit(solution)/shard_map/reduce_scatter | solution.py:115
Sparse Core Ops, SparseCore 0:
  22.1 36.7 all-reduce.6
  78.5 31.7 all-reduce.4
  117.2 21.8 reduce-scatter.2
  159.9 17.5 reduce-scatter.4
where the time goes:
time: 186 us; the launch traced here: 185 us
  waiting for transfers between devices  79.1 us (43%)
  blocking collectives  58.1 us (31%)
  matrix products  20.5 us (11%)
  between operations  14.5 us (8%)
  other arithmetic  7.73 us (4%)
  local copies, waits for them, and re-layouts  5.23 us (3%)
    psum x1, waiting for transfers between devices, on_device(): branch = lax.psum(branch_part, 'tp')  31.8 us
    unnamed x5, waiting for transfers between devices  20.1 us
    dot_general x9, matrix products, matmul(): return jnp.dot(left, right, preferred_element_type=jnp.float32)  19.5 us
    reduce_scatter x1, waiting for transfers between devices, on_device(): lax.psum_scatter(down_part.astype(jnp.bfloat16), 'tp', scatter_dimension=...  17.1 us
    all_gather x1, blocking collectives, on_device(): down_part = matmul(lax.all_gather(hidden, 'kv', axis=0, tiled=True), w_down)  14 us
    all_gather x1, blocking collectives, on_device(): lax.all_gather(heads.reshape(seq_local, width_v), 'kv', axis=0, tiled=True)  13.2 us
    psum x1, blocking collectives, on_device(): total_squares = lax.psum(part_squares, 'kv')  12.5 us
    unnamed x1, blocking collectives  11.9 us
  transfers between devices with their start and end apart: 4, of which 4 were waited for; matrix products, arithmetic and copies ran while one was open for 2% of the time, Pallas kernels for 0%

commit v1 on v0

--- a/solution.py
+++ b/solution.py
@@ -1,10 +1,15 @@
+import functools
+
 import jax
 import jax.numpy as jnp
 from jax import lax
+from jax.experimental import pallas as pl
+from jax.experimental.pallas import tpu as pltpu
 from jax.sharding import PartitionSpec as P
 
-D = 4096
-
+MESH = pl.DeviceIdType.MESH
+BF16 = jnp.bfloat16
+F32 = jnp.float32
 
 EPSILON = 1e-06
 
@@ -30,7 +35,7 @@
     return jnp.dot(left, right, preferred_element_type=jnp.float32)
 
 
-def on_device(
+def plain_on_device(
     tokens,
     gain_in,
     w_query,
@@ -53,6 +58,7 @@
     key_dim, value_dim = (cell_state.shape[2], cell_state.shape[3])
     head_start = lax.axis_index("tp") * head_count
     column_width = tokens.shape[1]
+    D = gain_in.shape[0] * lax.axis_size("kv")
     gathered = lax.all_gather(tokens, "tp", axis=1, tiled=True)
     widef = gathered.astype(jnp.float32)
     part_squares = jnp.sum(widef * widef, axis=1)
@@ -118,6 +124,469 @@
     residual = lax.dynamic_slice_in_dim(midf, lax.axis_index("tp") * column_width, column_width, 1)
     mixed = (residual + own_down).astype(jnp.bfloat16)
     return (mixed, cell_new, norm_new, max_new)
+
+
+class Exchange:
+    def __init__(self, sems):
+        self.send_sem, self.recv_sem = sems
+        self.used = 0
+        self.started = []
+
+    def copy(self, axis, target, src, dst):
+        index = self.used
+        self.used += 1
+        one = pltpu.make_async_remote_copy(
+            src_ref=src,
+            dst_ref=dst,
+            send_sem=self.send_sem.at[index],
+            recv_sem=self.recv_sem.at[index],
+            device_id={axis: target},
+            device_id_type=MESH,
+        )
+        one.start()
+        self.started.append(one)
+        return one
+
+
+def count_copies(kv, tp, subs):
+    return 3 * (tp - 1) + 4 * (kv - 1) + 2 * subs * (kv - 1)
+
+
+def layer_kernel(
+    kv,
+    tp,
+    subs,
+    tokens,
+    gain_in,
+    w_query,
+    w_key,
+    w_value,
+    w_outgate,
+    w_input_gate,
+    w_forget_gate,
+    bias_input,
+    bias_forget,
+    cell_state,
+    norm_state,
+    max_state,
+    w_proj,
+    gain_mid,
+    w_up,
+    w_down,
+    mixed,
+    cell_new,
+    norm_new,
+    max_new,
+    tok,
+    gain1,
+    wqkv,
+    wgi,
+    wgf,
+    bi,
+    bf,
+    cell,
+    norm,
+    mstate,
+    wproj,
+    gain2,
+    wup,
+    wdown,
+    out_v,
+    cell_o,
+    norm_o,
+    max_o,
+    terms,
+    b_send,
+    b_recv,
+    g_send,
+    g_recv,
+    numer,
+    h_all,
+    e_all,
+    sq_all,
+    mid,
+    nmid,
+    f_own,
+    f_send,
+    f_recv,
+    hid,
+    down,
+    d_send,
+    d_recv,
+    in_sem,
+    out_sem,
+    send_sem,
+    recv_sem,
+):
+    k_me, t_me = lax.axis_index("kv"), lax.axis_index("tp")
+    link = Exchange((send_sem, recv_sem))
+    rows, width = tok.shape[1], tok.shape[2]
+    own_rows, n_heads, key_dim, value_dim = cell.shape
+    wide = tp * width
+    total_width = kv * wide
+    w_qk, w_v = n_heads * key_dim, n_heads * value_dim
+    half = f_own.shape[2]
+    block = subs * half
+
+    loads = []
+
+    def load(src, dst):
+        one = pltpu.make_async_copy(src, dst, in_sem.at[len(loads)])
+        one.start()
+        loads.append(one)
+        return one
+
+    l_tok = load(tokens, tok.at[t_me])
+    l_gain = load(gain_in, gain1)
+    l_q = load(w_query, wqkv.at[:, 0:w_qk])
+    l_k = load(w_key, wqkv.at[:, w_qk : 2 * w_qk])
+    l_v = load(w_value, wqkv.at[:, 2 * w_qk : 2 * w_qk + w_v])
+    l_o = load(w_outgate, wqkv.at[:, 2 * w_qk + w_v : 2 * w_qk + 2 * w_v])
+    l_gates = [load(w_input_gate, wgi), load(w_forget_gate, wgf)]
+    l_small = [
+        load(bias_input, bi),
+        load(bias_forget, bf),
+        load(norm_state, norm),
+        load(max_state, mstate),
+    ]
+    l_cell = load(cell_state, cell)
+    l_proj = load(w_proj, wproj)
+    l_gain2 = load(gain_mid, gain2)
+    l_up = load(w_up, wup)
+    l_down = [
+        load(w_down.at[pl.ds(i * block, block)], wdown.at[pl.ds(i * block, block)])
+        for i in range(kv)
+    ]
+
+    barrier = pltpu.get_barrier_semaphore()
+    k_peers = [lax.rem(k_me + o, kv) for o in range(1, kv)]
+    t_peers = [lax.rem(t_me + o, tp) for o in range(1, tp)]
+    for peer in t_peers:
+        pl.semaphore_signal(barrier, inc=1, device_id={"tp": peer}, device_id_type=MESH)
+    for peer in k_peers:
+        pl.semaphore_signal(barrier, inc=1, device_id={"kv": peer}, device_id_type=MESH)
+    g_send[...] = jnp.zeros_like(g_send)
+    l_tok.wait()
+    pl.semaphore_wait(barrier, kv + tp - 2)
+
+    a_copies = [link.copy("tp", p, tok.at[t_me], tok.at[t_me]) for p in t_peers]
+    l_gain.wait()
+    for one in a_copies:
+        one.wait_recv()
+    wide_f = jnp.concatenate([tok[i] for i in range(tp)], axis=1).astype(F32)
+    squares = jnp.sum(wide_f * wide_f, axis=1, keepdims=True)
+    normed = (wide_f * gain1[...]).astype(BF16)
+
+    for one in l_gates:
+        one.wait()
+    n_gates = wgi.shape[1]
+    shape_g = (kv, own_rows, n_gates)
+    g_send[:, :, 0:n_gates] = matmul(normed, wgi[...]).reshape(shape_g)
+    g_send[:, :, 128 : 128 + n_gates] = matmul(normed, wgf[...]).reshape(shape_g)
+    g_send[:, :, 256:384] = jnp.broadcast_to(squares, (rows, 128)).reshape(kv, own_rows, 128)
+    g_copies = [
+        link.copy("kv", p, g_send.at[p], g_recv.at[o]) for o, p in enumerate(k_peers)
+    ]
+    for one in (l_q, l_k, l_v, l_o):
+        one.wait()
+    tile = 256
+
+    def project(i, carry):
+        cols = pl.ds(pl.multiple_of(i * tile, tile), tile)
+        part = matmul(normed, wqkv[:, cols]).reshape(kv, own_rows, tile)
+        terms[:, :, cols] = part
+        b_send[:, :, cols] = part.astype(BF16)
+        return carry
+
+    lax.fori_loop(0, wqkv.shape[1] // tile, project, 0)
+    b_copies = [
+        link.copy("kv", p, b_send.at[p], b_recv.at[o]) for o, p in enumerate(k_peers)
+    ]
+
+    for one in l_small:
+        one.wait()
+    l_cell.wait()
+    for one in g_copies:
+        one.wait_recv()
+    gates = g_send[k_me]
+    for o in range(kv - 1):
+        gates = gates + g_recv[o]
+    scale = lax.rsqrt(gates[:, 256:257] / total_width + EPSILON)
+    log_i = gates[:, 0:n_gates] * scale + bi[...]
+    raw_f = gates[:, 128 : 128 + n_gates] * scale + bf[...]
+    log_f = jnp.minimum(raw_f, 0.0) - jnp.log1p(jnp.exp(-jnp.abs(raw_f)))
+    gate_lane = lax.broadcasted_iota(jnp.int32, (own_rows, n_gates), 1)
+    keep, write, floor = [], [], []
+    for h in range(n_heads):
+        pick = gate_lane == t_me * n_heads + h
+        li = jnp.sum(jnp.where(pick, log_i, 0.0), axis=1, keepdims=True)
+        lf = jnp.sum(jnp.where(pick, log_f, 0.0), axis=1, keepdims=True)
+        old = mstate[:, h : h + 1]
+        new = jnp.maximum(lf + old, li)
+        max_o[:, h : h + 1] = new
+        keep.append(jnp.exp(lf + old - new))
+        write.append(jnp.exp(li - new))
+        floor.append(jnp.exp(-new))
+    outs = []
+
+    def store(src, dst):
+        one = pltpu.make_async_copy(src, dst, out_sem.at[len(outs)])
+        one.start()
+        outs.append(one)
+
+    store(max_o, max_new)
+    for one in b_copies:
+        one.wait_recv()
+    own = terms[k_me]
+    for o in range(kv - 1):
+        own = own + b_recv[o].astype(F32)
+    own = own * scale
+    query = own[:, 0:w_qk] * key_dim ** (-0.5)
+    keys = own[:, w_qk : 2 * w_qk]
+    values = own[:, 2 * w_qk : 2 * w_qk + w_v]
+    outgate = own[:, 2 * w_qk + w_v : 2 * w_qk + 2 * w_v]
+    qk_head = lax.broadcasted_iota(jnp.int32, (own_rows, w_qk), 1) // key_dim
+    spread = jnp.broadcast_to(write[0], (own_rows, w_qk))
+    for h in range(1, n_heads):
+        spread = jnp.where(qk_head == h, write[h], spread)
+    wkeys = keys * spread
+    pad = jnp.zeros((128 - 2 * own_rows, w_qk), F32)
+    turned = jnp.concatenate([wkeys, query, pad], axis=0).T
+    denom = []
+    for h in range(n_heads):
+        part = slice(h * key_dim, (h + 1) * key_dim)
+        fresh = keep[h] * norm[:, h, :] + wkeys[:, part]
+        norm_o[:, h, :] = fresh
+        dot = jnp.sum(query[:, part] * fresh, axis=1, keepdims=True)
+        denom.append(
+            jnp.broadcast_to(jnp.maximum(jnp.abs(dot), floor[h]), (own_rows, value_dim))
+        )
+    store(norm_o, norm_new)
+    for h in range(n_heads):
+        part = slice(h * key_dim, (h + 1) * key_dim)
+        vals = slice(h * value_dim, (h + 1) * value_dim)
+        for s in range(own_rows):
+            fresh = (
+                keep[h][s : s + 1, :] * cell[s, h]
+                + turned[part, s : s + 1] * values[s : s + 1, vals]
+            )
+            cell_o[s, h] = fresh
+            q_col = turned[part, own_rows + s : own_rows + s + 1]
+            numer[s : s + 1, vals] = jnp.sum(q_col * fresh, axis=0, keepdims=True)
+    heads = jax.nn.sigmoid(outgate) * numer[...] / jnp.concatenate(denom, axis=1)
+    h_all[k_me] = heads.astype(BF16)
+    h_copies = [link.copy("kv", p, h_all.at[k_me], h_all.at[k_me]) for p in k_peers]
+    store(cell_o, cell_new)
+    l_proj.wait()
+    for one in h_copies:
+        one.wait_recv()
+    all_heads = jnp.concatenate([h_all[i].astype(F32) for i in range(kv)], axis=0)
+
+    e_all[t_me] = matmul(all_heads.astype(BF16), wproj[...]).astype(BF16)
+    e_copies = [link.copy("tp", p, e_all.at[t_me], e_all.at[t_me]) for p in t_peers]
+    l_gain2.wait()
+    for one in e_copies:
+        one.wait_recv()
+    branch = e_all[0].astype(F32)
+    for i in range(1, tp):
+        branch = branch + e_all[i].astype(F32)
+    wide_f = jnp.concatenate([tok[i] for i in range(tp)], axis=1).astype(F32)
+    middle = (wide_f + branch).astype(BF16).astype(F32)
+    for i in range(tp):
+        mid[i] = middle[:, i * width : (i + 1) * width]
+    sq_all[k_me] = jnp.broadcast_to(jnp.sum(middle * middle, axis=1, keepdims=True), (rows, 128))
+    s_copies = [link.copy("kv", p, sq_all.at[k_me], sq_all.at[k_me]) for p in k_peers]
+    nmid[...] = (middle * gain2[...]).astype(BF16)
+
+    l_up.wait()
+    f_copies = {}
+    for sub in range(subs):
+        for o in list(range(1, kv)) + [0]:
+            peer = lax.rem(k_me + o, kv)
+            first = peer * block + sub * half
+
+            def raise_tile(i, carry, first=first, o=o, sub=sub):
+                cols = pl.ds(pl.multiple_of(first + i * tile, tile), tile)
+                here = pl.ds(pl.multiple_of(i * tile, tile), tile)
+                part = matmul(nmid[...], wup[:, cols])
+                if o:
+                    f_send[o - 1, sub, :, here] = part.astype(BF16)
+                else:
+                    f_own[sub, :, here] = part
+                return carry
+
+            lax.fori_loop(0, half // tile, raise_tile, 0)
+            if o:
+                f_copies[o, sub] = link.copy(
+                    "kv", peer, f_send.at[o - 1, sub], f_recv.at[o - 1, sub]
+                )
+    for one in s_copies:
+        one.wait_recv()
+    row_sum = sq_all[0, :, 0:1]
+    for i in range(1, kv):
+        row_sum = row_sum + sq_all[i, :, 0:1]
+    scale_mid = lax.rsqrt(row_sum / total_width + EPSILON)
+    g2_copies = {}
+    for sub in range(subs):
+        upward = f_own[sub]
+        for o in range(1, kv):
+            f_copies[o, sub].wait_recv()
+            upward = upward + f_recv[o - 1, sub].astype(F32)
+        hid[k_me, sub] = jnp.square(jnp.maximum(upward * scale_mid, 0.0)).astype(BF16)
+        for o in range(1, kv):
+            g2_copies[o, sub] = link.copy(
+                "kv", k_peers[o - 1], hid.at[k_me, sub], hid.at[k_me, sub]
+            )
+
+    for one in l_down:
+        one.wait()
+    for o in range(kv):
+        source = lax.rem(k_me + kv - o, kv)
+        for sub in range(subs):
+            if o:
+                g2_copies[o, sub].wait_recv()
+            deep = pl.ds(pl.multiple_of(source * block + sub * half, half), half)
+
+            def lower_tile(i, carry, source=source, sub=sub, deep=deep, o=o):
+                cols = pl.ds(pl.multiple_of(i * tile, tile), tile)
+                part = matmul(hid[source, sub], wdown[deep, cols])
+                if o or sub:
+                    part = part + down[:, cols]
+                down[:, cols] = part
+                return carry
+
+            lax.fori_loop(0, wide // tile, lower_tile, 0)
+    for i in range(tp):
+        d_send[i] = down[:, i * width : (i + 1) * width].astype(BF16)
+    d_copies = [
+        link.copy("tp", p, d_send.at[p], d_recv.at[o]) for o, p in enumerate(t_peers)
+    ]
+    lower = d_send[t_me].astype(F32)
+    for o, one in enumerate(d_copies):
+        one.wait_recv()
+        lower = lower + d_recv[o].astype(F32)
+    out_v[...] = (mid[t_me] + lower).astype(BF16)
+    store(out_v, mixed)
+    for one in link.started:
+        one.wait_send()
+    for one in outs:
+        one.wait()
+
+
+def fused_on_device(kv, tp, *args):
+    (tokens, gain_in, w_query, w_key, w_value, w_outgate, w_input_gate, w_forget_gate) = args[:8]
+    (bias_input, bias_forget, cell_state, norm_state, max_state) = args[8:13]
+    (w_proj, gain_mid, w_up, w_down) = args[13:]
+    rows, width = tokens.shape
+    own_rows = cell_state.shape[0]
+    wide = w_query.shape[0]
+    n_qkv = w_query.shape[1] + w_key.shape[1] + w_value.shape[1] + w_outgate.shape[1]
+    hidden = w_up.shape[1]
+    subs = 2
+    half = hidden // (kv * subs)
+    w_v = w_value.shape[1]
+    operands = (
+        tokens,
+        gain_in.reshape(1, -1),
+        w_query,
+        w_key,
+        w_value,
+        w_outgate,
+        w_input_gate,
+        w_forget_gate,
+        bias_input.reshape(1, -1),
+        bias_forget.reshape(1, -1),
+        cell_state,
+        norm_state,
+        max_state,
+        w_proj,
+        gain_mid.reshape(1, -1),
+        w_up,
+        w_down,
+    )
+    n_copies = count_copies(kv, tp, subs)
+    vm = pltpu.VMEM
+    scratch = [
+        vm((tp, rows, width), BF16),
+        vm((1, wide), F32),
+        vm((wide, n_qkv), BF16),
+        vm(w_input_gate.shape, BF16),
+        vm(w_forget_gate.shape, BF16),
+        vm((1, bias_input.shape[0]), F32),
+        vm((1, bias_forget.shape[0]), F32),
+        vm(cell_state.shape, F32),
+        vm(norm_state.shape, F32),
+        vm(max_state.shape, F32),
+        vm(w_proj.shape, BF16),
+        vm((1, wide), F32),
+        vm(w_up.shape, BF16),
+        vm(w_down.shape, BF16),
+        vm((rows, width), BF16),
+        vm(cell_state.shape, F32),
+        vm(norm_state.shape, F32),
+        vm(max_state.shape, F32),
+        vm((kv, own_rows, n_qkv), F32),
+        vm((kv, own_rows, n_qkv), BF16),
+        vm((kv - 1, own_rows, n_qkv), BF16),
+        vm((kv, own_rows, 384), F32),
+        vm((kv - 1, own_rows, 384), F32),
+        vm((own_rows, w_v), F32),
+        vm((kv, own_rows, w_v), BF16),
+        vm((tp, rows, wide), BF16),
+        vm((kv, rows, 128), F32),
+        vm((tp, rows, width), F32),
+        vm((rows, wide), BF16),
+        vm((subs, rows, half), F32),
+        vm((kv - 1, subs, rows, half), BF16),
+        vm((kv - 1, subs, rows, half), BF16),
+        vm((kv, subs, rows, half), BF16),
+        vm((rows, wide), F32),
+        vm((tp, rows, width), BF16),
+        vm((tp - 1, rows, width), BF16),
+        pltpu.SemaphoreType.DMA((16 + kv,)),
+        pltpu.SemaphoreType.DMA((4,)),
+        pltpu.SemaphoreType.DMA((n_copies,)),
+        pltpu.SemaphoreType.DMA((n_copies,)),
+    ]
+    anywhere = pl.BlockSpec(memory_space=pl.ANY)
+    return pl.pallas_call(
+        functools.partial(layer_kernel, kv, tp, subs),
+        out_shape=(
+            jax.ShapeDtypeStruct((rows, width), BF16),
+            jax.ShapeDtypeStruct(cell_state.shape, F32),
+            jax.ShapeDtypeStruct(norm_state.shape, F32),
+            jax.ShapeDtypeStruct(max_state.shape, F32),
+        ),
+        in_specs=[anywhere] * len(operands),
+        out_specs=(anywhere,) * 4,
+        scratch_shapes=scratch,
+        compiler_params=pltpu.CompilerParams(
+            collective_id=0, has_side_effects=True, vmem_limit_bytes=60 * 1024 * 1024
+        ),
+    )(*operands)
+
+
+def fits_kernel(kv, tp, *args):
+    tokens, w_query, cell_state, w_up = args[0], args[2], args[10], args[15]
+    return (
+        kv > 1
+        and tp > 1
+        and tokens.shape[1] % 128 == 0
+        and w_query.shape[0] % 256 == 0
+        and w_query.shape[1] % 256 == 0
+        and args[4].shape[1] % 256 == 0
+        and cell_state.shape[0] % 8 == 0
+        and 2 * cell_state.shape[0] <= 128
+        and cell_state.shape[3] % 128 == 0
+        and w_up.shape[1] % (512 * kv) == 0
+        and args[6].shape[1] <= 128
+    )
+
+
+def on_device(kv, tp, *args):
+    if fits_kernel(kv, tp, *args):
+        return fused_on_device(kv, tp, *args)
+    return plain_on_device(*args)
 
 
 def solution(mesh):
@@ -147,5 +616,6 @@
         P(("grp", "kv"), "tp"),
     )
     return jax.shard_map(
-        on_device, mesh=mesh, in_specs=in_specs, out_specs=out_specs, check_vma=False
-    )
+        functools.partial(on_device, mesh.shape["kv"], mesh.shape["tp"]),
+        mesh=mesh, in_specs=in_specs, out_specs=out_specs, check_vma=False
+    )

time: 186 us -> 55.7 us (0.30)
  waiting for transfers between devices: 79.1 us -> 0 us
  blocking collectives: 58.1 us -> 0 us
  Pallas kernels: 0 us -> 43.8 us
  matrix products: 20.5 us -> 0 us
  between operations: 14.5 us -> 0.64 us
  other arithmetic: 7.73 us -> 0 us
  local copies, waits for them, and re-layouts: 5.23 us -> 10.8 us
    pallas_call x0 -> x1, Pallas kernels: none -> 43.8 us  [fused_on_device(): pl.pallas_call(functools.partial(layer_kernel, kv, tp, subs), out_shape=(...]
    all_gather x3 -> x0, blocking collectives: 33.8 us -> none  [the longest x1 14 us: on_device(): down_part = matmul(lax.all_gather(hidden, 'kv', axis=0, tiled=True), w_down)]
    psum x1 -> x0, waiting for transfers between devices: 31.8 us -> none  [on_device(): branch = lax.psum(branch_part, 'tp')]
    reduce_scatter x2 -> x0, waiting for transfers between devices: 27.2 us -> none  [the longest x1 17.1 us: on_device(): lax.psum_scatter(down_part.astype(jnp.bfloat16), 'tp', scatter_dimension=...]
    dot_general x10 -> x0, matrix products: 20.5 us -> none  [the longest x9 19.5 us: matmul(): return jnp.dot(left, right, preferred_element_type=jnp.float32)]
    unnamed x5 -> x0, waiting for transfers between devices: 20.1 us -> none
    psum x1 -> x0, blocking collectives: 12.5 us -> none  [on_device(): total_squares = lax.psum(part_squares, 'kv')]
    unnamed x1 -> x0, blocking collectives: 11.9 us -> none
  transfers between devices with their start and end apart: 4 -> 0, of which waited for: 4 -> 0; matrix products, arithmetic and copies ran while one was open for 2% -> 0% of each run, Pallas kernels for 0% -> 0%
where the time goes in v1:
time: 55.7 us; the launch traced here: 55.2 us
  Pallas kernels  43.8 us (79%)
  local copies, waits for them, and re-layouts  10.8 us (19%)
  between operations  0.64 us (1%)
    pallas_call x1, Pallas kernels, fused_on_device(): pl.pallas_call(functools.partial(layer_kernel, kv, tp, subs), out_shape=(...  43.8 us
    unnamed x6, local copies, waits for them, and re-layouts  9.5 us
    pallas_call x1, local copies, waits for them, and re-layouts, fused_on_device(): pl.pallas_call(functools.partial(layer_kernel, kv, tp, subs), out_shape=(...  1.34 us

profile of v1, /device:TPU:0, one launch (start us, length us, event | category | flops | bytes accessed | tf_op | source)
XLA Modules:
  0.0 55.2 jit_solution(8634056538217262777)
XLA Ops:
  0.6 1.3 %copy.23.max_state = f32[8,4]{1,0:T(8,128)} copy(f32[8,4]{0,1:T(4,128)} %param.29) | data formatting | bytes 256 | tf_op args[12]
  2.0 1.6 %copy.21.w_input_gate = bf16[1024,16]{1,0:T(8,128)(2,1)} copy(bf16[1024,16]{0,1:T(8,128)(2,1)} %param.23) | data formatting | bytes 65536 | tf_op args[6]
  3.6 1.6 %copy.22.w_forget_gate = bf16[1024,16]{1,0:T(8,128)(2,1)} copy(bf16[1024,16]{0,1:T(8,128)(2,1)} %param.24) | data formatting | bytes 65536 | tf_op args[7]
  5.2 43.8 %shard_map.192 = (bf16[32,256]{1,0:T(8,128)(2,1)}, f32[8,4,64,128]{3,2,1,0:T(8,128)}, f32[8,4,64]{2,1,0:T(4,128)}, f32[8,4]{1,0:T(8,128)}) custom-call(bf16[32,256]{1,0:T(8,128)(2,1)} %tokens.1, f32[1,1024]{1,0:T(1,128)} %bitcast.4, bf16[1024,256]{1,0:T(8,128)(2,1)} %w_query.1, bf16[1024,256]{1,0:T(8,128)(2,1)} %w_key.1, bf16[1024,512]{1,0:T(8,128)(2,1)} %w_value.1, ...), custom_call_target="tpu_custom_call" | custom-call | tf_op jit(solution)/shard_map/pallas_call | solution.py:552
  49.0 1.3 %copy.24 = f32[8,4]{0,1:T(4,128)} copy(f32[8,4]{1,0:T(8,128)} %get-tuple-element.7) | data formatting | bytes 256 | tf_op jit(solution)/shard_map/pallas_call | solution.py:552
  50.3 1.3 %copy.28 = bf16[32,256]{1,0:T(8,128)(2,1)} copy(bf16[32,256]{1,0:T(8,128)(2,1)} %get-tuple-element.12) | data formatting | bytes 32768
  51.6 2.3 %copy.29 = f32[8,4,64,128]{3,2,1,0:T(8,128)} copy(f32[8,4,64,128]{3,2,1,0:T(8,128)} %get-tuple-element.13) | data formatting | bytes 2097152
  53.9 1.3 %copy.30 = f32[8,4,64]{2,1,0:T(4,128)} copy(f32[8,4,64]{2,1,0:T(4,128)} %get-tuple-element.14) | data formatting | bytes 16384

commit v2 on v1

--- a/solution.py
+++ b/solution.py
@@ -126,6 +126,10 @@
     return (mixed, cell_new, norm_new, max_new)
 
 
+def matmul_nt(left, right):
+    return lax.dot_general(left, right, (((1,), (1,)), ((), ())), preferred_element_type=F32)
+
+
 class Exchange:
     def __init__(self, sems):
         self.send_sem, self.recv_sem = sems
@@ -146,6 +150,15 @@
         one.start()
         self.started.append(one)
         return one
+
+
+def partners(me, count):
+    if count == 4:
+        both = [3 - me, lax.rem(me + 2, 4), me + 1 - 2 * lax.rem(me, 2)]
+        return both, both
+    ahead = [lax.rem(me + o, count) for o in range(1, count)]
+    behind = [lax.rem(me + count - o, count) for o in range(1, count)]
+    return ahead, behind
 
 
 def count_copies(kv, tp, subs):
@@ -259,8 +272,8 @@
     ]
 
     barrier = pltpu.get_barrier_semaphore()
-    k_peers = [lax.rem(k_me + o, kv) for o in range(1, kv)]
-    t_peers = [lax.rem(t_me + o, tp) for o in range(1, tp)]
+    k_peers, k_from = partners(k_me, kv)
+    t_peers, t_from = partners(t_me, tp)
     for peer in t_peers:
         pl.semaphore_signal(barrier, inc=1, device_id={"tp": peer}, device_id_type=MESH)
     for peer in k_peers:
@@ -279,10 +292,10 @@
 
     for one in l_gates:
         one.wait()
-    n_gates = wgi.shape[1]
+    n_gates = wgi.shape[0]
     shape_g = (kv, own_rows, n_gates)
-    g_send[:, :, 0:n_gates] = matmul(normed, wgi[...]).reshape(shape_g)
-    g_send[:, :, 128 : 128 + n_gates] = matmul(normed, wgf[...]).reshape(shape_g)
+    g_send[:, :, 0:n_gates] = matmul_nt(normed, wgi[...]).reshape(shape_g)
+    g_send[:, :, 128 : 128 + n_gates] = matmul_nt(normed, wgf[...]).reshape(shape_g)
     g_send[:, :, 256:384] = jnp.broadcast_to(squares, (rows, 128)).reshape(kv, own_rows, 128)
     g_copies = [
         link.copy("kv", p, g_send.at[p], g_recv.at[o]) for o, p in enumerate(k_peers)
@@ -317,13 +330,15 @@
     log_f = jnp.minimum(raw_f, 0.0) - jnp.log1p(jnp.exp(-jnp.abs(raw_f)))
     gate_lane = lax.broadcasted_iota(jnp.int32, (own_rows, n_gates), 1)
     keep, write, floor = [], [], []
+    max_cols = []
+    old_max = mstate[...].T
     for h in range(n_heads):
         pick = gate_lane == t_me * n_heads + h
         li = jnp.sum(jnp.where(pick, log_i, 0.0), axis=1, keepdims=True)
         lf = jnp.sum(jnp.where(pick, log_f, 0.0), axis=1, keepdims=True)
-        old = mstate[:, h : h + 1]
+        old = old_max[:, h : h + 1]
         new = jnp.maximum(lf + old, li)
-        max_o[:, h : h + 1] = new
+        max_cols.append(new)
         keep.append(jnp.exp(lf + old - new))
         write.append(jnp.exp(li - new))
         floor.append(jnp.exp(-new))
@@ -334,6 +349,11 @@
         one.start()
         outs.append(one)
 
+    head_lane = lax.broadcasted_iota(jnp.int32, (own_rows, n_heads), 1)
+    new_max = jnp.broadcast_to(max_cols[0], (own_rows, n_heads))
+    for h in range(1, n_heads):
+        new_max = jnp.where(head_lane == h, max_cols[h], new_max)
+    max_o[...] = new_max.T
     store(max_o, max_new)
     for one in b_copies:
         one.wait_recv()
@@ -352,30 +372,38 @@
     wkeys = keys * spread
     pad = jnp.zeros((128 - 2 * own_rows, w_qk), F32)
     turned = jnp.concatenate([wkeys, query, pad], axis=0).T
-    denom = []
+    denom, cross = [], []
     for h in range(n_heads):
         part = slice(h * key_dim, (h + 1) * key_dim)
         fresh = keep[h] * norm[:, h, :] + wkeys[:, part]
         norm_o[:, h, :] = fresh
         dot = jnp.sum(query[:, part] * fresh, axis=1, keepdims=True)
-        denom.append(
-            jnp.broadcast_to(jnp.maximum(jnp.abs(dot), floor[h]), (own_rows, value_dim))
-        )
+        shape_v = (own_rows, value_dim)
+        denom.append(jnp.broadcast_to(jnp.maximum(jnp.abs(dot), floor[h]), shape_v))
+        dot = jnp.sum(query[:, part] * wkeys[:, part], axis=1, keepdims=True)
+        cross.append(jnp.broadcast_to(dot, shape_v))
+    for h in range(n_heads):
+        part = slice(h * key_dim, (h + 1) * key_dim)
+        vals = slice(h * value_dim, (h + 1) * value_dim)
+        for s in range(own_rows):
+            q_col = turned[part, own_rows + s : own_rows + s + 1]
+            numer[s : s + 1, vals] = jnp.sum(q_col * cell[s, h], axis=0, keepdims=True)
+    keep_v = jnp.concatenate(
+        [jnp.broadcast_to(one, (own_rows, value_dim)) for one in keep], axis=1
+    )
+    above = keep_v * numer[...] + jnp.concatenate(cross, axis=1) * values
+    heads = jax.nn.sigmoid(outgate) * above / jnp.concatenate(denom, axis=1)
+    h_all[k_me] = heads.astype(BF16)
+    h_copies = [link.copy("kv", p, h_all.at[k_me], h_all.at[k_me]) for p in k_peers]
     store(norm_o, norm_new)
     for h in range(n_heads):
         part = slice(h * key_dim, (h + 1) * key_dim)
         vals = slice(h * value_dim, (h + 1) * value_dim)
         for s in range(own_rows):
-            fresh = (
+            cell_o[s, h] = (
                 keep[h][s : s + 1, :] * cell[s, h]
                 + turned[part, s : s + 1] * values[s : s + 1, vals]
             )
-            cell_o[s, h] = fresh
-            q_col = turned[part, own_rows + s : own_rows + s + 1]
-            numer[s : s + 1, vals] = jnp.sum(q_col * fresh, axis=0, keepdims=True)
-    heads = jax.nn.sigmoid(outgate) * numer[...] / jnp.concatenate(denom, axis=1)
-    h_all[k_me] = heads.astype(BF16)
-    h_copies = [link.copy("kv", p, h_all.at[k_me], h_all.at[k_me]) for p in k_peers]
     store(cell_o, cell_new)
     l_proj.wait()
     for one in h_copies:
@@ -400,26 +428,31 @@
 
     l_up.wait()
     f_copies = {}
+
+    def raise_block(target, sub, put):
+        first = target * block + sub * half
+
+        def raise_tile(i, carry):
+            cols = pl.ds(pl.multiple_of(first + i * tile, tile), tile)
+            put(pl.ds(pl.multiple_of(i * tile, tile), tile), matmul(nmid[...], wup[:, cols]))
+            return carry
+
+        lax.fori_loop(0, half // tile, raise_tile, 0)
+
     for sub in range(subs):
-        for o in list(range(1, kv)) + [0]:
-            peer = lax.rem(k_me + o, kv)
-            first = peer * block + sub * half
-
-            def raise_tile(i, carry, first=first, o=o, sub=sub):
-                cols = pl.ds(pl.multiple_of(first + i * tile, tile), tile)
-                here = pl.ds(pl.multiple_of(i * tile, tile), tile)
-                part = matmul(nmid[...], wup[:, cols])
-                if o:
-                    f_send[o - 1, sub, :, here] = part.astype(BF16)
-                else:
-                    f_own[sub, :, here] = part
-                return carry
-
-            lax.fori_loop(0, half // tile, raise_tile, 0)
-            if o:
-                f_copies[o, sub] = link.copy(
-                    "kv", peer, f_send.at[o - 1, sub], f_recv.at[o - 1, sub]
-                )
+        for o, peer in enumerate(k_peers):
+
+            def put_sent(here, part, o=o, sub=sub):
+                f_send[o, sub, :, here] = part.astype(BF16)
+
+            raise_block(peer, sub, put_sent)
+            f_copies[o, sub] = link.copy("kv", peer, f_send.at[o, sub], f_recv.at[o, sub])
+    for sub in range(subs):
+
+        def put_own(here, part, sub=sub):
+            f_own[sub, :, here] = part
+
+        raise_block(k_me, sub, put_own)
     for one in s_copies:
         one.wait_recv()
     row_sum = sq_all[0, :, 0:1]
@@ -429,33 +462,27 @@
     g2_copies = {}
     for sub in range(subs):
         upward = f_own[sub]
-        for o in range(1, kv):
+        for o in range(kv - 1):
             f_copies[o, sub].wait_recv()
-            upward = upward + f_recv[o - 1, sub].astype(F32)
+            upward = upward + f_recv[o, sub].astype(F32)
         hid[k_me, sub] = jnp.square(jnp.maximum(upward * scale_mid, 0.0)).astype(BF16)
-        for o in range(1, kv):
-            g2_copies[o, sub] = link.copy(
-                "kv", k_peers[o - 1], hid.at[k_me, sub], hid.at[k_me, sub]
-            )
+        for o, peer in enumerate(k_peers):
+            g2_copies[o, sub] = link.copy("kv", peer, hid.at[k_me, sub], hid.at[k_me, sub])
 
     for one in l_down:
         one.wait()
-    for o in range(kv):
-        source = lax.rem(k_me + kv - o, kv)
-        for sub in range(subs):
-            if o:
-                g2_copies[o, sub].wait_recv()
-            deep = pl.ds(pl.multiple_of(source * block + sub * half, half), half)
-
-            def lower_tile(i, carry, source=source, sub=sub, deep=deep, o=o):
-                cols = pl.ds(pl.multiple_of(i * tile, tile), tile)
-                part = matmul(hid[source, sub], wdown[deep, cols])
-                if o or sub:
-                    part = part + down[:, cols]
-                down[:, cols] = part
-                return carry
-
-            lax.fori_loop(0, wide // tile, lower_tile, 0)
+
+    def lower_block(source, sub, first):
+        deep = pl.ds(pl.multiple_of(source * block + sub * half, half), half)
+        part = matmul(hid[source, sub], wdown[deep, :])
+        down[...] = part if first else down[...] + part
+
+    for sub in range(subs):
+        lower_block(k_me, sub, sub == 0)
+    for sub in range(subs):
+        for o in list(range(kv - 1))[::-1]:
+            g2_copies[o, sub].wait_recv()
+            lower_block(k_from[o], sub, False)
     for i in range(tp):
         d_send[i] = down[:, i * width : (i + 1) * width].astype(BF16)
     d_copies = [
@@ -473,6 +500,23 @@
         one.wait()
 
 
+def finish_kernel(*refs):
+    sources, outs, stage = refs[0:4], refs[4:8], refs[8:12]
+    in_sem, out_sem = refs[12:]
+    pieces = [(sources[i], stage[i], outs[i]) for i in (0, 2, 3)]
+    for s in range(sources[1].shape[0]):
+        pieces.append((sources[1].at[s], stage[1].at[s], outs[1].at[s]))
+    inward = [pltpu.make_async_copy(p[0], p[1], in_sem.at[i]) for i, p in enumerate(pieces)]
+    outward = [pltpu.make_async_copy(p[1], p[2], out_sem.at[i]) for i, p in enumerate(pieces)]
+    for one in inward:
+        one.start()
+    for one, two in zip(inward, outward):
+        one.wait()
+        two.start()
+    for two in outward:
+        two.wait()
+
+
 def fused_on_device(kv, tp, *args):
     (tokens, gain_in, w_query, w_key, w_value, w_outgate, w_input_gate, w_forget_gate) = args[:8]
     (bias_input, bias_forget, cell_state, norm_state, max_state) = args[8:13]
@@ -482,7 +526,7 @@
     wide = w_query.shape[0]
     n_qkv = w_query.shape[1] + w_key.shape[1] + w_value.shape[1] + w_outgate.shape[1]
     hidden = w_up.shape[1]
-    subs = 2
+    subs = 4 if hidden % (1024 * kv) == 0 else 2
     half = hidden // (kv * subs)
     w_v = w_value.shape[1]
     operands = (
@@ -492,13 +536,13 @@
         w_key,
         w_value,
         w_outgate,
-        w_input_gate,
-        w_forget_gate,
+        w_input_gate.T,
+        w_forget_gate.T,
         bias_input.reshape(1, -1),
         bias_forget.reshape(1, -1),
         cell_state,
         norm_state,
-        max_state,
+        max_state.T,
         w_proj,
         gain_mid.reshape(1, -1),
         w_up,
@@ -510,13 +554,13 @@
         vm((tp, rows, width), BF16),
         vm((1, wide), F32),
         vm((wide, n_qkv), BF16),
-        vm(w_input_gate.shape, BF16),
-        vm(w_forget_gate.shape, BF16),
+        vm(w_input_gate.shape[::-1], BF16),
+        vm(w_forget_gate.shape[::-1], BF16),
         vm((1, bias_input.shape[0]), F32),
         vm((1, bias_forget.shape[0]), F32),
         vm(cell_state.shape, F32),
         vm(norm_state.shape, F32),
-        vm(max_state.shape, F32),
+        vm(max_state.shape[::-1], F32),
         vm(w_proj.shape, BF16),
         vm((1, wide), F32),
         vm(w_up.shape, BF16),
@@ -524,7 +568,7 @@
         vm((rows, width), BF16),
         vm(cell_state.shape, F32),
         vm(norm_state.shape, F32),
-        vm(max_state.shape, F32),
+        vm(max_state.shape[::-1], F32),
         vm((kv, own_rows, n_qkv), F32),
         vm((kv, own_rows, n_qkv), BF16),
         vm((kv - 1, own_rows, n_qkv), BF16),
@@ -549,13 +593,13 @@
         pltpu.SemaphoreType.DMA((n_copies,)),
     ]
     anywhere = pl.BlockSpec(memory_space=pl.ANY)
-    return pl.pallas_call(
+    results = pl.pallas_call(
         functools.partial(layer_kernel, kv, tp, subs),
         out_shape=(
             jax.ShapeDtypeStruct((rows, width), BF16),
             jax.ShapeDtypeStruct(cell_state.shape, F32),
             jax.ShapeDtypeStruct(norm_state.shape, F32),
-            jax.ShapeDtypeStruct(max_state.shape, F32),
+            jax.ShapeDtypeStruct(max_state.shape[::-1], F32),
         ),
         in_specs=[anywhere] * len(operands),
         out_specs=(anywhere,) * 4,
@@ -564,6 +608,16 @@
             collective_id=0, has_side_effects=True, vmem_limit_bytes=60 * 1024 * 1024
         ),
     )(*operands)
+    mixed, cell_new, norm_new, max_new = pl.pallas_call(
+        finish_kernel,
+        out_shape=tuple(jax.ShapeDtypeStruct(one.shape, one.dtype) for one in results),
+        in_specs=[anywhere] * 4,
+        out_specs=(anywhere,) * 4,
+        scratch_shapes=[vm(one.shape, one.dtype) for one in results]
+        + [pltpu.SemaphoreType.DMA((3 + own_rows,))] * 2,
+        compiler_params=pltpu.CompilerParams(vmem_limit_bytes=60 * 1024 * 1024),
+    )(*results)
+    return (mixed, cell_new, norm_new, max_new.T)
 
 
 def fits_kernel(kv, tp, *args):

time: 55.7 us -> 45.3 us (0.81)
  local copies, waits for them, and re-layouts: 10.8 us -> 0 us
    unnamed x6 -> x0, local copies, waits for them, and re-layouts: 9.5 us -> none
    pallas_call x0 -> x1, Pallas kernels: none -> 2.17 us  [fused_on_device(): pl.pallas_call(finish_kernel, out_shape=tuple((jax.ShapeDtypeStruct(one.s...]
    pallas_call x1, Pallas kernels: 43.8 us -> 42.1 us  [fused_on_device(): pl.pallas_call(functools.partial(layer_kernel, kv, tp, subs), out_shape=(...]
    pallas_call x1 -> x0, local copies, waits for them, and re-layouts: 1.34 us -> none  [fused_on_device(): pl.pallas_call(functools.partial(layer_kernel, kv, tp, subs), out_shape=(...]
where the time goes in v2:
time: 45.3 us; the launch traced here: 44.9 us
  Pallas kernels  44.3 us (98%)
  between operations  0.65 us (1%)
    pallas_call x1, Pallas kernels, fused_on_device(): pl.pallas_call(functools.partial(layer_kernel, kv, tp, subs), out_shape=(...  42.1 us
    pallas_call x1, Pallas kernels, fused_on_device(): pl.pallas_call(finish_kernel, out_shape=tuple((jax.ShapeDtypeStruct(one.s...  2.17 us

profile of v2, /device:TPU:0, one launch (start us, length us, event | category | flops | bytes accessed | tf_op | source)
XLA Modules:
  0.0 44.9 jit_solution(4489535079317288415)
XLA Ops:
  0.6 42.1 %shard_map.192 = (bf16[32,256]{1,0:T(8,128)(2,1)}, f32[8,4,64,128]{3,2,1,0:T(8,128)}, f32[8,4,64]{2,1,0:T(4,128)}, f32[4,8]{1,0:T(4,128)}) custom-call(bf16[32,256]{1,0:T(8,128)(2,1)} %tokens.1, f32[1,1024]{1,0:T(1,128)} %bitcast.10, bf16[1024,256]{1,0:T(8,128)(2,1)} %w_query.1, bf16[1024,256]{1,0:T(8,128)(2,1)} %w_key.1, bf16[1024,512]{1,0:T(8,128)(2,1)} %w_value.1, ...), custom_call_target="tpu_custom_call" | custom-call | tf_op jit(solution)/shard_map/pallas_call | solution.py:596
  42.8 2.2 %shard_map.193 = (bf16[32,256]{1,0:T(8,128)(2,1)}, f32[8,4,64,128]{3,2,1,0:T(8,128)}, f32[8,4,64]{2,1,0:T(4,128)}, f32[4,8]{1,0:T(4,128)}) custom-call(bf16[32,256]{1,0:T(8,128)(2,1)} %get-tuple-element.12.refs_0_, f32[8,4,64,128]{3,2,1,0:T(8,128)} %get-tuple-element.13.refs_1_, f32[8,4,64]{2,1,0:T(4,128)} %get-tuple-element.14.refs_2_, ...), custom_call_target="tpu_custom_call" | custom-call | tf_op jit(solution)/shard_map/pallas_call | solution.py:611

commit v3 on v2

--- a/solution.py
+++ b/solution.py
@@ -136,7 +136,7 @@
         self.used = 0
         self.started = []
 
-    def copy(self, axis, target, src, dst):
+    def copy(self, axis, target, src, dst, when=None):
         index = self.used
         self.used += 1
         one = pltpu.make_async_remote_copy(
@@ -147,7 +147,10 @@
             device_id={axis: target},
             device_id_type=MESH,
         )
-        one.start()
+        if when is None:
+            one.start()
+        else:
+            pl.when(when)(one.start)
         self.started.append(one)
         return one
 
@@ -262,14 +265,6 @@
         load(norm_state, norm),
         load(max_state, mstate),
     ]
-    l_cell = load(cell_state, cell)
-    l_proj = load(w_proj, wproj)
-    l_gain2 = load(gain_mid, gain2)
-    l_up = load(w_up, wup)
-    l_down = [
-        load(w_down.at[pl.ds(i * block, block)], wdown.at[pl.ds(i * block, block)])
-        for i in range(kv)
-    ]
 
     barrier = pltpu.get_barrier_semaphore()
     k_peers, k_from = partners(k_me, kv)
@@ -283,6 +278,14 @@
     pl.semaphore_wait(barrier, kv + tp - 2)
 
     a_copies = [link.copy("tp", p, tok.at[t_me], tok.at[t_me]) for p in t_peers]
+    l_cell = load(cell_state, cell)
+    l_proj = load(w_proj, wproj)
+    l_gain2 = load(gain_mid, gain2)
+    l_up = load(w_up, wup)
+    l_down = [
+        load(w_down.at[pl.ds(i * block, block)], wdown.at[pl.ds(i * block, block)])
+        for i in range(kv)
+    ]
     l_gain.wait()
     for one in a_copies:
         one.wait_recv()
@@ -439,15 +442,33 @@
 
         lax.fori_loop(0, half // tile, raise_tile, 0)
 
-    for sub in range(subs):
-        for o, peer in enumerate(k_peers):
+    is_end = jnp.logical_or(k_me == 0, k_me == kv - 1)
+    is_mid = jnp.logical_not(is_end)
+    across, skip, near = k_peers
+    targets = [across, jnp.where(is_end, near, skip), near]
+    for o in (1, 0, 2):
+        for sub in range(subs):
 
             def put_sent(here, part, o=o, sub=sub):
                 f_send[o, sub, :, here] = part.astype(BF16)
 
-            raise_block(peer, sub, put_sent)
-            f_copies[o, sub] = link.copy("kv", peer, f_send.at[o, sub], f_recv.at[o, sub])
+            raise_block(k_peers[o], sub, put_sent)
+            f_copies[o, sub] = link.copy(
+                "kv",
+                targets[o],
+                f_send.at[o, sub],
+                f_recv.at[o, sub],
+                when=None if o else is_end,
+            )
     for sub in range(subs):
+        f_copies[1, sub].wait_recv()
+
+        def relay(sub=sub):
+            both = f_send[0, sub].astype(F32) + f_recv[1, sub].astype(F32)
+            f_send[0, sub] = both.astype(BF16)
+            f_copies[0, sub].start()
+
+        pl.when(is_mid)(relay)
 
         def put_own(here, part, sub=sub):
             f_own[sub, :, here] = part
@@ -462,12 +483,17 @@
     g2_copies = {}
     for sub in range(subs):
         upward = f_own[sub]
-        for o in range(kv - 1):
-            f_copies[o, sub].wait_recv()
-            upward = upward + f_recv[o, sub].astype(F32)
+        f_copies[0, sub].wait_recv()
+        f_copies[2, sub].wait_recv()
+        skipped = jnp.where(is_end, f_recv[1, sub].astype(F32), 0.0)
+        upward = upward + f_recv[0, sub].astype(F32) + skipped + f_recv[2, sub].astype(F32)
         hid[k_me, sub] = jnp.square(jnp.maximum(upward * scale_mid, 0.0)).astype(BF16)
-        for o, peer in enumerate(k_peers):
-            g2_copies[o, sub] = link.copy("kv", peer, hid.at[k_me, sub], hid.at[k_me, sub])
+        mine = hid.at[k_me, sub]
+        g2_copies[0, sub] = link.copy("kv", across, mine, mine)
+        carried = hid.at[jnp.where(is_end, k_me, across), sub]
+        to = jnp.where(is_end, skip, near)
+        g2_copies[1, sub] = link.copy("kv", to, carried, carried, when=is_end)
+        g2_copies[2, sub] = link.copy("kv", near, mine, mine)
 
     for one in l_down:
         one.wait()
@@ -480,9 +506,14 @@
     for sub in range(subs):
         lower_block(k_me, sub, sub == 0)
     for sub in range(subs):
-        for o in list(range(kv - 1))[::-1]:
-            g2_copies[o, sub].wait_recv()
-            lower_block(k_from[o], sub, False)
+        g2_copies[0, sub].wait_recv()
+        pl.when(is_mid)(g2_copies[1, sub].start)
+        lower_block(across, sub, False)
+        g2_copies[2, sub].wait_recv()
+        lower_block(near, sub, False)
+    for sub in range(subs):
+        g2_copies[1, sub].wait_recv()
+        lower_block(skip, sub, False)
     for i in range(tp):
         d_send[i] = down[:, i * width : (i + 1) * width].astype(BF16)
     d_copies = [
@@ -623,7 +654,7 @@
 def fits_kernel(kv, tp, *args):
     tokens, w_query, cell_state, w_up = args[0], args[2], args[10], args[15]
     return (
-        kv > 1
+        kv == 4
         and tp > 1
         and tokens.shape[1] % 128 == 0
         and w_query.shape[0] % 256 == 0

time: 45.3 us -> 45.5 us (level)
  no operation moved by 1% of the time
where the time goes in v3:
time: 45.5 us; the launch traced here: 45.1 us
  Pallas kernels  44.5 us (98%)
  between operations  0.65 us (1%)
    pallas_call x1, Pallas kernels, fused_on_device(): pl.pallas_call(functools.partial(layer_kernel, kv, tp, subs), out_shape=(...  42.3 us
    pallas_call x1, Pallas kernels, fused_on_device(): pl.pallas_call(finish_kernel, out_shape=tuple((jax.ShapeDtypeStruct(one.s...  2.17 us

profile of v3, /device:TPU:0, one launch (start us, length us, event | category | flops | bytes accessed | tf_op | source)
XLA Modules:
  0.0 45.1 jit_solution(1207661399354012245)
XLA Ops:
  0.6 42.3 %shard_map.192 = (bf16[32,256]{1,0:T(8,128)(2,1)}, f32[8,4,64,128]{3,2,1,0:T(8,128)}, f32[8,4,64]{2,1,0:T(4,128)}, f32[4,8]{1,0:T(4,128)}) custom-call(bf16[32,256]{1,0:T(8,128)(2,1)} %tokens.1, f32[1,1024]{1,0:T(1,128)} %bitcast.10, bf16[1024,256]{1,0:T(8,128)(2,1)} %w_query.1, bf16[1024,256]{1,0:T(8,128)(2,1)} %w_key.1, bf16[1024,512]{1,0:T(8,128)(2,1)} %w_value.1, ...), custom_call_target="tpu_custom_call" | custom-call | tf_op jit(solution)/shard_map/pallas_call | solution.py:627
  43.0 2.2 %shard_map.193 = (bf16[32,256]{1,0:T(8,128)(2,1)}, f32[8,4,64,128]{3,2,1,0:T(8,128)}, f32[8,4,64]{2,1,0:T(4,128)}, f32[4,8]{1,0:T(4,128)}) custom-call(bf16[32,256]{1,0:T(8,128)(2,1)} %get-tuple-element.12.refs_0_, f32[8,4,64,128]{3,2,1,0:T(8,128)} %get-tuple-element.13.refs_1_, f32[8,4,64]{2,1,0:T(4,128)} %get-tuple-element.14.refs_2_, ...), custom_call_target="tpu_custom_call" | custom-call | tf_op jit(solution)/shard_map/pallas_call | solution.py:642

commit v4 on v3

--- a/solution.py
+++ b/solution.py
@@ -165,7 +165,7 @@
 
 
 def count_copies(kv, tp, subs):
-    return 3 * (tp - 1) + 4 * (kv - 1) + 2 * subs * (kv - 1)
+    return 3 * (tp - 1) + 5 * (kv - 1) + 2 * subs * (kv - 1)
 
 
 def layer_kernel(
@@ -189,10 +189,10 @@
     gain_mid,
     w_up,
     w_down,
-    mixed,
-    cell_new,
-    norm_new,
-    max_new,
+    out_v,
+    cell_o,
+    norm_o,
+    max_o,
     tok,
     gain1,
     wqkv,
@@ -207,10 +207,6 @@
     gain2,
     wup,
     wdown,
-    out_v,
-    cell_o,
-    norm_o,
-    max_o,
     terms,
     b_send,
     b_recv,
@@ -230,7 +226,6 @@
     d_send,
     d_recv,
     in_sem,
-    out_sem,
     send_sem,
     recv_sem,
 ):
@@ -314,10 +309,14 @@
         b_send[:, :, cols] = part.astype(BF16)
         return carry
 
-    lax.fori_loop(0, wqkv.shape[1] // tile, project, 0)
-    b_copies = [
-        link.copy("kv", p, b_send.at[p], b_recv.at[o]) for o, p in enumerate(k_peers)
-    ]
+    n_tiles = wqkv.shape[1] // tile
+    b_copies = []
+    for low, high in ((0, n_tiles // 2), (n_tiles // 2, n_tiles)):
+        lax.fori_loop(low, high, project, 0)
+        cols = pl.ds(low * tile, (high - low) * tile)
+        for o, p in enumerate(k_peers):
+            here = b_send.at[p, :, cols], b_recv.at[o, :, cols]
+            b_copies.append(link.copy("kv", p, *here))
 
     for one in l_small:
         one.wait()
@@ -345,19 +344,11 @@
         keep.append(jnp.exp(lf + old - new))
         write.append(jnp.exp(li - new))
         floor.append(jnp.exp(-new))
-    outs = []
-
-    def store(src, dst):
-        one = pltpu.make_async_copy(src, dst, out_sem.at[len(outs)])
-        one.start()
-        outs.append(one)
-
     head_lane = lax.broadcasted_iota(jnp.int32, (own_rows, n_heads), 1)
     new_max = jnp.broadcast_to(max_cols[0], (own_rows, n_heads))
     for h in range(1, n_heads):
         new_max = jnp.where(head_lane == h, max_cols[h], new_max)
     max_o[...] = new_max.T
-    store(max_o, max_new)
     for one in b_copies:
         one.wait_recv()
     own = terms[k_me]
@@ -398,7 +389,6 @@
     heads = jax.nn.sigmoid(outgate) * above / jnp.concatenate(denom, axis=1)
     h_all[k_me] = heads.astype(BF16)
     h_copies = [link.copy("kv", p, h_all.at[k_me], h_all.at[k_me]) for p in k_peers]
-    store(norm_o, norm_new)
     for h in range(n_heads):
         part = slice(h * key_dim, (h + 1) * key_dim)
         vals = slice(h * value_dim, (h + 1) * value_dim)
@@ -407,7 +397,6 @@
                 keep[h][s : s + 1, :] * cell[s, h]
                 + turned[part, s : s + 1] * values[s : s + 1, vals]
             )
-    store(cell_o, cell_new)
     l_proj.wait()
     for one in h_copies:
         one.wait_recv()
@@ -489,11 +478,8 @@
         upward = upward + f_recv[0, sub].astype(F32) + skipped + f_recv[2, sub].astype(F32)
         hid[k_me, sub] = jnp.square(jnp.maximum(upward * scale_mid, 0.0)).astype(BF16)
         mine = hid.at[k_me, sub]
-        g2_copies[0, sub] = link.copy("kv", across, mine, mine)
-        carried = hid.at[jnp.where(is_end, k_me, across), sub]
-        to = jnp.where(is_end, skip, near)
-        g2_copies[1, sub] = link.copy("kv", to, carried, carried, when=is_end)
-        g2_copies[2, sub] = link.copy("kv", near, mine, mine)
+        for o, peer in enumerate(k_peers):
+            g2_copies[o, sub] = link.copy("kv", peer, mine, mine)
 
     for one in l_down:
         one.wait()
@@ -506,14 +492,9 @@
     for sub in range(subs):
         lower_block(k_me, sub, sub == 0)
     for sub in range(subs):
-        g2_copies[0, sub].wait_recv()
-        pl.when(is_mid)(g2_copies[1, sub].start)
-        lower_block(across, sub, False)
-        g2_copies[2, sub].wait_recv()
-        lower_block(near, sub, False)
-    for sub in range(subs):
-        g2_copies[1, sub].wait_recv()
-        lower_block(skip, sub, False)
+        for o in (2, 1, 0):
+            g2_copies[o, sub].wait_recv()
+            lower_block(k_from[o], sub, False)
     for i in range(tp):
         d_send[i] = down[:, i * width : (i + 1) * width].astype(BF16)
     d_copies = [
@@ -524,28 +505,17 @@
         one.wait_recv()
         lower = lower + d_recv[o].astype(F32)
     out_v[...] = (mid[t_me] + lower).astype(BF16)
-    store(out_v, mixed)
     for one in link.started:
         one.wait_send()
-    for one in outs:
+
+
+def finish_kernel(*refs):
+    sources, outs, sem = refs[0:4], refs[4:8], refs[8]
+    copies = [pltpu.make_async_copy(sources[i], outs[i], sem.at[i]) for i in range(4)]
+    for one in copies:
+        one.start()
+    for one in copies:
         one.wait()
-
-
-def finish_kernel(*refs):
-    sources, outs, stage = refs[0:4], refs[4:8], refs[8:12]
-    in_sem, out_sem = refs[12:]
-    pieces = [(sources[i], stage[i], outs[i]) for i in (0, 2, 3)]
-    for s in range(sources[1].shape[0]):
-        pieces.append((sources[1].at[s], stage[1].at[s], outs[1].at[s]))
-    inward = [pltpu.make_async_copy(p[0], p[1], in_sem.at[i]) for i, p in enumerate(pieces)]
-    outward = [pltpu.make_async_copy(p[1], p[2], out_sem.at[i]) for i, p in enumerate(pieces)]
-    for one in inward:
-        one.start()
-    for one, two in zip(inward, outward):
-        one.wait()
-        two.start()
-    for two in outward:
-        two.wait()
 
 
 def fused_on_device(kv, tp, *args):
@@ -560,7 +530,7 @@
     subs = 4 if hidden % (1024 * kv) == 0 else 2
     half = hidden // (kv * subs)
     w_v = w_value.shape[1]
-    operands = (
+    operands = tuple(pltpu.with_memory_space_constraint(x, pltpu.HBM) for x in (
         tokens,
         gain_in.reshape(1, -1),
         w_query,
@@ -578,7 +548,7 @@
         gain_mid.reshape(1, -1),
         w_up,
         w_down,
-    )
+    ))
     n_copies = count_copies(kv, tp, subs)
     vm = pltpu.VMEM
     scratch = [
@@ -596,10 +566,6 @@
         vm((1, wide), F32),
         vm(w_up.shape, BF16),
         vm(w_down.shape, BF16),
-        vm((rows, width), BF16),
-        vm(cell_state.shape, F32),
-        vm(norm_state.shape, F32),
-        vm(max_state.shape[::-1], F32),
         vm((kv, own_rows, n_qkv), F32),
         vm((kv, own_rows, n_qkv), BF16),
         vm((kv - 1, own_rows, n_qkv), BF16),
@@ -619,11 +585,11 @@
         vm((tp, rows, width), BF16),
         vm((tp - 1, rows, width), BF16),
         pltpu.SemaphoreType.DMA((16 + kv,)),
-        pltpu.SemaphoreType.DMA((4,)),
         pltpu.SemaphoreType.DMA((n_copies,)),
         pltpu.SemaphoreType.DMA((n_copies,)),
     ]
-    anywhere = pl.BlockSpec(memory_space=pl.ANY)
+    anywhere = pl.BlockSpec(memory_space=pltpu.HBM)
+    in_vmem = pl.BlockSpec(memory_space=pltpu.VMEM)
     results = pl.pallas_call(
         functools.partial(layer_kernel, kv, tp, subs),
         out_shape=(
@@ -633,20 +599,19 @@
             jax.ShapeDtypeStruct(max_state.shape[::-1], F32),
         ),
         in_specs=[anywhere] * len(operands),
-        out_specs=(anywhere,) * 4,
+        out_specs=(in_vmem,) * 4,
         scratch_shapes=scratch,
         compiler_params=pltpu.CompilerParams(
-            collective_id=0, has_side_effects=True, vmem_limit_bytes=60 * 1024 * 1024
+            collective_id=0, has_side_effects=True, vmem_limit_bytes=36 * 1024 * 1024
         ),
     )(*operands)
     mixed, cell_new, norm_new, max_new = pl.pallas_call(
         finish_kernel,
         out_shape=tuple(jax.ShapeDtypeStruct(one.shape, one.dtype) for one in results),
-        in_specs=[anywhere] * 4,
+        in_specs=[in_vmem] * 4,
         out_specs=(anywhere,) * 4,
-        scratch_shapes=[vm(one.shape, one.dtype) for one in results]
-        + [pltpu.SemaphoreType.DMA((3 + own_rows,))] * 2,
-        compiler_params=pltpu.CompilerParams(vmem_limit_bytes=60 * 1024 * 1024),
+        scratch_shapes=[pltpu.SemaphoreType.DMA((4,))],
+        compiler_params=pltpu.CompilerParams(vmem_limit_bytes=8 * 1024 * 1024),
     )(*results)
     return (mixed, cell_new, norm_new, max_new.T)
 

time: 45.5 us -> 41.6 us (0.914)
  Pallas kernels: 44.5 us -> 40.7 us
    pallas_call x1, Pallas kernels: 42.3 us -> 39.7 us  [fused_on_device(): pl.pallas_call(functools.partial(layer_kernel, kv, tp, subs), out_shape=(...]
    pallas_call x1, Pallas kernels: 2.17 us -> 1.02 us  [fused_on_device(): pl.pallas_call(finish_kernel, out_shape=tuple((jax.ShapeDtypeStruct(one.s...]
where the time goes in v4:
time: 41.6 us; the launch traced here: 41.4 us
  Pallas kernels  40.7 us (98%)
  between operations  0.65 us (2%)
    pallas_call x1, Pallas kernels, fused_on_device(): pl.pallas_call(functools.partial(layer_kernel, kv, tp, subs), out_shape=(...  39.7 us
    pallas_call x1, Pallas kernels, fused_on_device(): pl.pallas_call(finish_kernel, out_shape=tuple((jax.ShapeDtypeStruct(one.s...  1.02 us

profile of v4, /device:TPU:0, one launch (start us, length us, event | category | flops | bytes accessed | tf_op | source)
XLA Modules:
  0.0 41.4 jit_solution(11197015269140442434)
XLA Ops:
  0.6 39.7 %shard_map.192 = (bf16[32,256]{1,0:T(8,128)(2,1)S(1)}, f32[8,4,64,128]{3,2,1,0:T(8,128)S(1)}, f32[8,4,64]{2,1,0:T(4,128)S(1)}, f32[4,8]{1,0:T(4,128)S(1)}) custom-call(bf16[32,256]{1,0:T(8,128)(2,1)} %tokens.1, f32[1,1024]{1,0:T(1,128)} %bitcast.10, bf16[1024,256]{1,0:T(8,128)(2,1)} %w_query.1, bf16[1024,256]{1,0:T(8,128)(2,1)} %w_key.1, ...), custom_call_target="tpu_custom_call" | custom-call | tf_op jit(solution)/shard_map/pallas_call | solution.py:593
  40.4 1.0 %shard_map.193 = (bf16[32,256]{1,0:T(8,128)(2,1)}, f32[8,4,64,128]{3,2,1,0:T(8,128)}, f32[8,4,64]{2,1,0:T(4,128)}, f32[4,8]{1,0:T(4,128)}) custom-call(bf16[32,256]{1,0:T(8,128)(2,1)S(1)} %get-tuple-element.12.refs_0_, f32[8,4,64,128]{3,2,1,0:T(8,128)S(1)} %get-tuple-element.13.refs_1_, f32[8,4,64]{2,1,0:T(4,128)S(1)} %get-tuple-element.14.refs_2_, ...), custom_call_target="tpu_custom_call" | custom-call | tf_op jit(solution)/shard_map/pallas_call | solution.py:608

commit v5 on v4

--- a/solution.py
+++ b/solution.py
@@ -300,20 +300,13 @@
     ]
     for one in (l_q, l_k, l_v, l_o):
         one.wait()
-    tile = 256
-
-    def project(i, carry):
-        cols = pl.ds(pl.multiple_of(i * tile, tile), tile)
-        part = matmul(normed, wqkv[:, cols]).reshape(kv, own_rows, tile)
-        terms[:, :, cols] = part
-        b_send[:, :, cols] = part.astype(BF16)
-        return carry
-
-    n_tiles = wqkv.shape[1] // tile
+    n_qkv = wqkv.shape[1]
     b_copies = []
-    for low, high in ((0, n_tiles // 2), (n_tiles // 2, n_tiles)):
-        lax.fori_loop(low, high, project, 0)
-        cols = pl.ds(low * tile, (high - low) * tile)
+    for low, high in ((0, n_qkv // 2), (n_qkv // 2, n_qkv)):
+        part = matmul(normed, wqkv[:, low:high]).reshape(kv, own_rows, high - low)
+        terms[:, :, low:high] = part
+        b_send[:, :, low:high] = part.astype(BF16)
+        cols = pl.ds(low, high - low)
         for o, p in enumerate(k_peers):
             here = b_send.at[p, :, cols], b_recv.at[o, :, cols]
             b_copies.append(link.copy("kv", p, *here))
@@ -421,34 +414,28 @@
     l_up.wait()
     f_copies = {}
 
-    def raise_block(target, sub, put):
-        first = target * block + sub * half
-
-        def raise_tile(i, carry):
-            cols = pl.ds(pl.multiple_of(first + i * tile, tile), tile)
-            put(pl.ds(pl.multiple_of(i * tile, tile), tile), matmul(nmid[...], wup[:, cols]))
-            return carry
-
-        lax.fori_loop(0, half // tile, raise_tile, 0)
+    pair = 2
+
+    def raise_block(target, sub):
+        first = pl.multiple_of(target * block + sub * half, half)
+        return matmul(nmid[...], wup[:, pl.ds(first, pair * half)])
 
     is_end = jnp.logical_or(k_me == 0, k_me == kv - 1)
     is_mid = jnp.logical_not(is_end)
     across, skip, near = k_peers
     targets = [across, jnp.where(is_end, near, skip), near]
     for o in (1, 0, 2):
-        for sub in range(subs):
-
-            def put_sent(here, part, o=o, sub=sub):
-                f_send[o, sub, :, here] = part.astype(BF16)
-
-            raise_block(k_peers[o], sub, put_sent)
-            f_copies[o, sub] = link.copy(
-                "kv",
-                targets[o],
-                f_send.at[o, sub],
-                f_recv.at[o, sub],
-                when=None if o else is_end,
-            )
+        for low in range(0, subs, pair):
+            part = raise_block(k_peers[o], low).astype(BF16)
+            for sub in range(low, low + pair):
+                f_send[o, sub] = part[:, (sub - low) * half : (sub - low + 1) * half]
+                f_copies[o, sub] = link.copy(
+                    "kv",
+                    targets[o],
+                    f_send.at[o, sub],
+                    f_recv.at[o, sub],
+                    when=None if o else is_end,
+                )
     for sub in range(subs):
         f_copies[1, sub].wait_recv()
 
@@ -458,11 +445,10 @@
             f_copies[0, sub].start()
 
         pl.when(is_mid)(relay)
-
-        def put_own(here, part, sub=sub):
-            f_own[sub, :, here] = part
-
-        raise_block(k_me, sub, put_own)
+        if sub % pair == 0:
+            part = raise_block(k_me, sub)
+            for i in range(pair):
+                f_own[sub + i] = part[:, i * half : (i + 1) * half]
     for one in s_copies:
         one.wait_recv()
     row_sum = sq_all[0, :, 0:1]

time: 41.6 us -> 41.7 us (level)
  no operation moved by 1% of the time
where the time goes in v5:
time: 41.7 us; the launch traced here: 41.4 us
  Pallas kernels  40.8 us (98%)
  between operations  0.65 us (2%)
    pallas_call x1, Pallas kernels, fused_on_device(): pl.pallas_call(functools.partial(layer_kernel, kv, tp, subs), out_shape=(...  39.8 us
    pallas_call x1, Pallas kernels, fused_on_device(): pl.pallas_call(finish_kernel, out_shape=tuple((jax.ShapeDtypeStruct(one.s...  1.02 us

profile of v5, /device:TPU:0, one launch (start us, length us, event | category | flops | bytes accessed | tf_op | source)
XLA Modules:
  0.0 41.4 jit_solution(2147780322552263)
XLA Ops:
  0.6 39.8 %shard_map.192 = (bf16[32,256]{1,0:T(8,128)(2,1)S(1)}, f32[8,4,64,128]{3,2,1,0:T(8,128)S(1)}, f32[8,4,64]{2,1,0:T(4,128)S(1)}, f32[4,8]{1,0:T(4,128)S(1)}) custom-call(bf16[32,256]{1,0:T(8,128)(2,1)} %tokens.1, f32[1,1024]{1,0:T(1,128)} %bitcast.10, bf16[1024,256]{1,0:T(8,128)(2,1)} %w_query.1, bf16[1024,256]{1,0:T(8,128)(2,1)} %w_key.1, ...), custom_call_target="tpu_custom_call" | custom-call | tf_op jit(solution)/shard_map/pallas_call | solution.py:579
  40.4 1.0 %shard_map.193 = (bf16[32,256]{1,0:T(8,128)(2,1)}, f32[8,4,64,128]{3,2,1,0:T(8,128)}, f32[8,4,64]{2,1,0:T(4,128)}, f32[4,8]{1,0:T(4,128)}) custom-call(bf16[32,256]{1,0:T(8,128)(2,1)S(1)} %get-tuple-element.12.refs_0_, f32[8,4,64,128]{3,2,1,0:T(8,128)S(1)} %get-tuple-element.13.refs_1_, f32[8,4,64]{2,1,0:T(4,128)S(1)} %get-tuple-element.14.refs_2_, ...), custom_call_target="tpu_custom_call" | custom-call | tf_op jit(solution)/shard_map/pallas_call | solution.py:594
